TPU v7x, 32 devices: a whole 2x2x4 slice. The times are simulated.
32 devices in a mesh: grp: 2 (over y), sp: 4 (over z), tp: 4 (over x, core).
Axes of the slice: x: 2, y: 2, z: 4, core: 2. Of those that a mesh axis runs over, the one named last changes fastest.
Arguments:
- stream: bfloat16 [6144, 4096], P(('grp', 'sp'), 'tp'), parts along dimension 0, may hold values from -400 to 400
- in_weight: bfloat16 [2, 1024, 4096], P(None, 'sp', 'tp'), may hold values from -0.09375 to 0.09375
- out_weight: bfloat16 [2, 1024, 4096], P(None, 'sp', 'tp'), may hold values from -0.1875 to 0.1875
- group_mix: bfloat16 [2, 4, 256, 256], replicated, may hold values from -0.375 to 0.375
- pool_gain: float32 [2, 1024], replicated, may hold values from 0.1 to 1.9
- norm_gain: float32 [2, 4096], P(None, 'tp'), may hold values from 0.1 to 1.9
- norm_shift: float32 [2, 4096], P(None, 'tp'), may hold values from -3 to 3
Outputs:
- refined: bfloat16 [6144, 4096], P(('grp', 'sp'), 'tp'), parts along dimension 0
There are 2 independent parts, one for each index of `grp`. A program takes and returns all parts, laid end to end along the dimension named above; an argument that names none is the same for every part. Nothing has to cross between parts.
All inputs are finite; a program needn't handle non-finite values.
Results may differ from a plain program's by a relative error of at most 0.015.
Values may be sent and summed in bfloat16 or wider, within the bound.
A program may use at most 64 MiB of HBM per device.

v0:
```python
import jax
import jax.numpy as jnp
from jax import lax
from jax.sharding import PartitionSpec as P

D = 4096
POOL = 1024
GROUPS = 4
GROUP_WIDTH = 256
LAYERS = 2


epsilon = 1e-05


def passed_along(block, axis, distance):
    devices = range(lax.axis_size(axis))
    route = [(i - distance, i) for i in devices if i - distance in devices]
    return lax.ppermute(block, axis, route)


def pooled_windows(hidden, tok_start):
    reach = 2**GROUPS - 1
    length = hidden.shape[1]
    channels = hidden.shape[0]
    earlier = passed_along(hidden[:, length - reach :], "sp", 1)
    extended = jnp.concatenate([earlier, hidden], axis=1).astype(jnp.float32)
    group_ids = (jnp.arange(channels, dtype=jnp.int32) // GROUP_WIDTH)[:, None]
    running = extended
    window_sums = jnp.zeros((channels, length), jnp.float32)
    for octave in range(GROUPS):
        offset = 2**octave
        running = running[:, offset:] + running[:, : running.shape[1] - offset]
        window_sums = jnp.where(
            group_ids == octave, running[:, running.shape[1] - length :], window_sums
        )
    positions = (tok_start + jnp.arange(length, dtype=jnp.int32) + 1).astype(jnp.float32)
    widths = jnp.exp2((group_ids + 1).astype(jnp.float32))
    counts = jnp.minimum(positions[None, :], widths)
    return (window_sums / counts - hidden.astype(jnp.float32)).astype(jnp.bfloat16)


def per_device(stream, in_weight, out_weight, group_mix, pool_gain, norm_gain, norm_shift):
    tok_rows = stream.shape[0]
    tok_start = lax.axis_index("sp") * tok_rows
    alpha = (2.0 * LAYERS) ** 0.25
    contract_rows = (((0,), (0,)), ((), ()))
    contract_cols = (((1,), (1,)), ((), ()))
    current = stream
    for layer_index in range(LAYERS):
        whole_in = lax.all_gather(in_weight[layer_index], "sp", axis=0, tiled=True)
        partial_value = lax.dot_general(
            whole_in, current, contract_cols, preferred_element_type=jnp.float32
        )
        hidden = lax.psum(partial_value.astype(jnp.bfloat16), "tp")
        pooled = pooled_windows(hidden, tok_start)
        grouped = pooled.reshape(GROUPS, GROUP_WIDTH, tok_rows)
        mixed = jnp.einsum(
            "gio,git->got", group_mix[layer_index], grouped, preferred_element_type=jnp.float32
        )
        gains = pool_gain[layer_index].reshape(GROUPS, GROUP_WIDTH, 1)
        scaled = (mixed * gains).astype(jnp.bfloat16).reshape(POOL, tok_rows)
        branch = lax.dot_general(
            scaled,
            lax.all_gather(out_weight[layer_index], "sp", axis=0, tiled=True),
            contract_rows,
            preferred_element_type=jnp.float32,
        )
        summed = alpha * current.astype(jnp.float32) + branch
        row_sum, row_squares = lax.psum(
            (jnp.sum(summed, axis=1), jnp.sum(summed * summed, axis=1)), "tp"
        )
        row_mean = row_sum / D
        row_var = row_squares / D - row_mean * row_mean
        normed = (summed - row_mean[:, None]) * lax.rsqrt(row_var + epsilon)[:, None]
        current = (
            normed * norm_gain[layer_index][None, :] + norm_shift[layer_index][None, :]
        ).astype(jnp.bfloat16)
    return current


def solution(mesh):
    in_specs = (
        P(("grp", "sp"), "tp"),
        P(None, "sp", "tp"),
        P(None, "sp", "tp"),
        P(),
        P(),
        P(None, "tp"),
        P(None, "tp"),
    )
    out_specs = P(("grp", "sp"), "tp")
    return jax.shard_map(
        per_device, mesh=mesh, in_specs=in_specs, out_specs=out_specs, check_vma=False
    )
```

profile of v0, /device:TPU:0, one launch (start us, length us, event | category | flops | bytes accessed | tf_op | source)
XLA Modules:
  0.0 312.8 jit_solution(13905823871252964514)
XLA Ops:
  6.5 2.2 fusion.49
  8.9 48.5 %all-gather.9.cloned.1.call-done = bf16[1,1024,1024]{2,1,0:T(8,128)(2,1)} async-done(((bf16[1,256,1024]{2,1,0:T(8,128)(2,1)}), bf16[1,1024,1024]{2,1,0:T(8,128)(2,1)}) %all-gather.9.cloned.1.call-update) | async-done | bytes 2097168 | tf_op jit(solution)/shard_map/all_gather | solution.py:51
  57.3 5.0 %fusion.22 = bf16[1024,768]{1,0:T(8,128)(2,1)} fusion(bf16[768,1024]{1,0:T(8,128)(2,1)} %param.7, bf16[1,1024,1024]{2,1,0:T(8,128)(2,1)} %all-gather.9.cloned.1.call-done), kind=kOutput, calls=%fused_computation.40 | convolution fusion | flops 1611399168 | bytes 5242880 | tf_op jit(solution)/shard_map/dot_general | solution.py:52
  62.4 1.1 fusion.48
  64.3 39.9 %all-reduce.5.cloned.1.call-done = bf16[1024,768]{1,0:T(8,128)(2,1)} async-done(((bf16[1024,768]{1,0:T(8,128)(2,1)}), bf16[1024,768]{1,0:T(8,128)(2,1)}) %all-reduce.5.cloned.1.call-update) | async-done | bytes 1572880 | tf_op jit(solution)/shard_map/psum | solution.py:55
  104.2 1.1 slice.138
  105.3 3.4 %collective-permute-start = (bf16[1024,15]{1,0:T(8,128)(2,1)S(1)}, bf16[1024,15]{1,0:T(8,128)(2,1)S(1)}, u32[]{:S(2)}, u32[]{:S(2)}) collective-permute-start(bf16[1024,15]{1,0:T(8,128)(2,1)S(1)} %slice.138), channel_id=1, source_target_pairs={{0,4},{4,8},{8,12},{1,5},{5,9},{9,13},{2,6},{6,10},{10,14},{3,7},{... | collective-permute-start | bytes 92168 | tf_op jit(solution)/shard_map/ppermute | solution.py:19
  108.7 5.4 %collective-permute-done = bf16[1024,15]{1,0:T(8,128)(2,1)S(1)} collective-permute-done((bf16[1024,15]{1,0:T(8,128)(2,1)S(1)}, bf16[1024,15]{1,0:T(8,128)(2,1)S(1)}, u32[]{:S(2)}, u32[]{:S(2)}) %collective-permute-start) | collective-permute-done | bytes 30752 | tf_op jit(solution)/shard_map/ppermute | solution.py:19
  114.1 2.3 maximum_convert_fusion
  116.4 1.0 slice_add_fusion.5
  117.4 1.0 slice_add_fusion.4
  118.5 1.0 slice_add_fusion.3
  119.9 4.1 %fusion.1 = bf16[1024,768]{1,0:T(8,128)(2,1)S(1)} fusion(f32[1024,782]{1,0:T(8,128)S(1)} %slice_add_fusion.5, f32[1024,780]{1,0:T(8,128)S(1)} %slice_add_fusion.4, f32[1024,776]{1,0:T(8,128)S(1)} %slice_add_fusion.3, bf16[1024,768]{1,0:T(8,128)(2,1)S(1)} %copy-done, f32[1024]{0:T(1024)S(1)} %fusion.44, f32[768]{0:T(1024)S(1)} %add_convert_fusion.2, ...), kind=kLoop, calls=%fused_computation.9 | loop fusion | flops 7864320 | bytes 15739904 | tf_op jit(solution)/shard_map/convert_element_type | solution.py:40
  124.7 26.8 %all-gather.11.cloned.1.call-done = bf16[1,1024,1024]{2,1,0:T(8,128)(2,1)} async-done(((bf16[1,256,1024]{2,1,0:T(8,128)(2,1)}), bf16[1,1024,1024]{2,1,0:T(8,128)(2,1)}) %all-gather.11.cloned.1.call-update) | async-done | bytes 2097168 | tf_op jit(solution)/shard_map/all_gather | solution.py:65
  151.5 5.8 %fusion.47 = (f32[768]{0:T(1024)S(1)}, f32[768]{0:T(1024)S(1)}, f32[768,1024]{1,0:T(8,128)}) fusion(bf16[1024,768]{1,0:T(8,128)(2,1)S(1)} %bitcast.56, bf16[1,1024,1024]{2,1,0:T(8,128)(2,1)} %all-gather.11.cloned.1.call-done, bf16[768,1024]{1,0:T(8,128)(2,1)} %param.7), kind=kOutput, calls=%fused_computation.70 | convolution fusion | flops 1615329792 | bytes 8394752 | tf_op jit(solution)/shard_map/dot_general | solution.py:63
  157.3 6.5 %all-reduce.1 = (f32[768]{0:T(1024)S(1)}, f32[768]{0:T(1024)S(1)}) all-reduce(f32[768]{0:T(1024)S(1)} %get-tuple-element.8, f32[768]{0:T(1024)S(1)} %get-tuple-element.7), channel_id=1, replica_groups=mesh['grp'=2,'sp'=4,'tp'=4] {'tp'}, use_global_device_ids=true, to_apply=%region_4.5 | all-reduce | flops 1536 | bytes 12288 | tf_op jit(solution)/shard_map/psum | solution.py:70
  163.8 33.6 %all-gather.13.cloned.1.call-done = bf16[1,1024,1024]{2,1,0:T(8,128)(2,1)} async-done(((bf16[1,256,1024]{2,1,0:T(8,128)(2,1)}), bf16[1,1024,1024]{2,1,0:T(8,128)(2,1)}) %all-gather.13.cloned.1.call-update) | async-done | bytes 2097168 | tf_op jit(solution)/shard_map/all_gather | solution.py:51
  197.4 5.6 %fusion.28 = bf16[1024,768]{1,0:T(8,128)(2,1)} fusion(bf16[1,1024,1024]{2,1,0:T(8,128)(2,1)} %all-gather.13.cloned.1.call-done, f32[768,1024]{1,0:T(8,128)} %get-tuple-element.27, f32[1024]{0:T(1024)S(1)} %bitcast.61, f32[1024]{0:T(1024)S(1)} %bitcast.59, f32[768]{0:T(1024)S(1)} %get-tuple-element.26, f32[768]{0:T(1024)S(1)} %get-tuple-element.25), kind=kOutput, calls=%fused_computation.42 | convolution fusion | flops 1615331328 | bytes 6830080 | tf_op jit(solution)/shard_map/dot_general | solution.py:52
  203.7 41.2 %all-reduce.7.cloned.1.call-done = bf16[1024,768]{1,0:T(8,128)(2,1)} async-done(((bf16[1024,768]{1,0:T(8,128)(2,1)}), bf16[1024,768]{1,0:T(8,128)(2,1)}) %all-reduce.7.cloned.1.call-update) | async-done | bytes 1572880 | tf_op jit(solution)/shard_map/psum | solution.py:55
  244.9 1.1 slice.149
  246.0 3.6 %collective-permute-start.1 = (bf16[1024,15]{1,0:T(8,128)(2,1)S(1)}, bf16[1024,15]{1,0:T(8,128)(2,1)S(1)}, u32[]{:S(2)}, u32[]{:S(2)}) collective-permute-start(bf16[1024,15]{1,0:T(8,128)(2,1)S(1)} %slice.149), channel_id=1, source_target_pairs={{0,4},{4,8},{8,12},{1,5},{5,9},{9,13},{2,6},{6,10},{10,14},{3,7},{... | collective-permute-start | bytes 92168 | tf_op jit(solution)/shard_map/ppermute | solution.py:19
  249.6 5.5 %collective-permute-done.1 = bf16[1024,15]{1,0:T(8,128)(2,1)S(1)} collective-permute-done((bf16[1024,15]{1,0:T(8,128)(2,1)S(1)}, bf16[1024,15]{1,0:T(8,128)(2,1)S(1)}, u32[]{:S(2)}, u32[]{:S(2)}) %collective-permute-start.1) | collective-permute-done | bytes 30752 | tf_op jit(solution)/shard_map/ppermute | solution.py:19
  255.2 2.2 maximum_convert_fusion.1
  257.4 1.0 slice_add_fusion.2
  258.4 1.0 slice_add_fusion.1
  259.4 1.0 slice_add_fusion
  260.9 4.1 %fusion.3 = bf16[1024,768]{1,0:T(8,128)(2,1)S(1)} fusion(f32[1024,782]{1,0:T(8,128)S(1)} %slice_add_fusion.2, f32[1024,780]{1,0:T(8,128)S(1)} %slice_add_fusion.1, f32[1024,776]{1,0:T(8,128)S(1)} %slice_add_fusion, bf16[1024,768]{1,0:T(8,128)(2,1)S(1)} %copy-done.1, f32[1024]{0:T(1024)S(1)} %fusion.44, f32[768]{0:T(1024)S(1)} %add_convert_fusion.2, ...), kind=kLoop, calls=%fused_computation.11 | loop fusion | flops 7864320 | bytes 15739904 | tf_op jit(solution)/shard_map/convert_element_type | solution.py:40
  265.0 1.8 multiply_convert_fusion
  266.8 25.3 %all-gather.15.cloned.1.call-done = bf16[1,1024,1024]{2,1,0:T(8,128)(2,1)} async-done(((bf16[1,256,1024]{2,1,0:T(8,128)(2,1)}), bf16[1,1024,1024]{2,1,0:T(8,128)(2,1)}) %all-gather.15.cloned.1.call-update) | async-done | bytes 2097168 | tf_op jit(solution)/shard_map/all_gather | solution.py:65
  292.1 5.6 %fusion.46 = (f32[768]{0:T(1024)S(1)}, f32[768]{0:T(1024)S(1)}, f32[768,1024]{1,0:T(8,128)S(1)}) fusion(bf16[1024,768]{1,0:T(8,128)(2,1)} %bitcast.55, bf16[1,1024,1024]{2,1,0:T(8,128)(2,1)} %all-gather.15.cloned.1.call-done, f32[1024]{0:T(1024)S(1)} %bitcast.62, f32[1024]{0:T(1024)S(1)} %bitcast.60, f32[768]{0:T(1024)S(1)} %get-tuple-element.26, ...), kind=kOutput, calls=%fused_computation.69 | convolution fusion | flops 1619261952 | bytes 9981952 | tf_op jit(solution)/shard_map/dot_general | solution.py:63
  297.7 6.5 %all-reduce = (f32[768]{0:T(1024)S(1)}, f32[768]{0:T(1024)S(1)}) all-reduce(f32[768]{0:T(1024)S(1)} %get-tuple-element.6, f32[768]{0:T(1024)S(1)} %get-tuple-element.5), channel_id=1, replica_groups=mesh['grp'=2,'sp'=4,'tp'=4] {'tp'}, use_global_device_ids=true, to_apply=%region_9.10 | all-reduce | flops 1536 | bytes 12288 | tf_op jit(solution)/shard_map/psum | solution.py:70
  304.2 1.7 add_convert_fusion
  (38 shorter events, 2.9 us)
Async XLA Ops:
  6.5 50.8 %all-gather.9.cloned.1.call-start = ((), (), s32[]{:S(2)}) async-start(), calls=%async_computation.2 | async-start | bytes 2621440 | tf_op jit(solution)/shard_map/all_gather | solution.py:51
  8.8 53.6 %copy-start.2 = (bf16[2,256,1024]{2,1,0:T(8,128)(2,1)S(1)}, bf16[2,256,1024]{2,1,0:T(8,128)(2,1)}, u32[]{:S(2)}) copy-start(bf16[2,256,1024]{2,1,0:T(8,128)(2,1)} %param.9) | copy-start | bytes 3145732
  8.8 95.4 %all-reduce.5.cloned.1.call-start = ((), (), s32[]{:S(2)}) async-start(), calls=%async_computation | async-start | bytes 3145728 | tf_op jit(solution)/shard_map/psum | solution.py:55
  62.3 1.9 copy-start.4
  62.3 1.9 copy-start.5
  62.3 1.9 copy-start.6
  62.4 89.1 %all-gather.11.cloned.1.call-start = ((), (), s32[]{:S(2)}) async-start(), calls=%async_computation.3 | async-start | bytes 2621440 | tf_op jit(solution)/shard_map/all_gather | solution.py:65
  63.5 133.9 %all-gather.13.cloned.1.call-start = ((), (), s32[]{:S(2)}) async-start(), calls=%async_computation.4 | async-start | bytes 2621440 | tf_op jit(solution)/shard_map/all_gather | solution.py:51
  64.1 180.8 %all-reduce.7.cloned.1.call-start = ((), (), s32[]{:S(2)}) async-start(), calls=%async_computation.1 | async-start | bytes 3145728 | tf_op jit(solution)/shard_map/psum | solution.py:55
  105.3 8.8 %collective-permute-start = (bf16[1024,15]{1,0:T(8,128)(2,1)S(1)}, bf16[1024,15]{1,0:T(8,128)(2,1)S(1)}, u32[]{:S(2)}, u32[]{:S(2)}) collective-permute-start(bf16[1024,15]{1,0:T(8,128)(2,1)S(1)} %slice.138), channel_id=1, source_target_pairs={{0,4},{4,8},{8,12},{1,5},{5,9},{9,13},{2,6},{6,10},{10,14},{3,7},{... | collective-permute-start | bytes 92168 | tf_op jit(solution)/shard_map/ppermute | solution.py:19
  118.5 1.4 copy-start
  119.9 4.1 %copy-start.3 = (bf16[2,4,256,256]{3,2,1,0:T(8,128)(2,1)S(1)}, bf16[2,4,256,256]{3,2,1,0:T(8,128)(2,1)}, u32[]{:S(2)}) copy-start(bf16[2,4,256,256]{3,2,1,0:T(8,128)(2,1)} %param.10) | copy-start | bytes 3145732
  203.1 89.0 %all-gather.15.cloned.1.call-start = ((), (), s32[]{:S(2)}) async-start(), calls=%async_computation.5 | async-start | bytes 2621440 | tf_op jit(solution)/shard_map/all_gather | solution.py:65
  246.0 9.2 %collective-permute-start.1 = (bf16[1024,15]{1,0:T(8,128)(2,1)S(1)}, bf16[1024,15]{1,0:T(8,128)(2,1)S(1)}, u32[]{:S(2)}, u32[]{:S(2)}) collective-permute-start(bf16[1024,15]{1,0:T(8,128)(2,1)S(1)} %slice.149), channel_id=1, source_target_pairs={{0,4},{4,8},{8,12},{1,5},{5,9},{9,13},{2,6},{6,10},{10,14},{3,7},{... | collective-permute-start | bytes 92168 | tf_op jit(solution)/shard_map/ppermute | solution.py:19
  259.4 1.4 copy-start.1
Sparse Core Ops, SparseCore 0:
  8.9 48.3 all-gather.8
  62.5 41.6 all-reduce.4
  105.8 45.7 all-gather.10
  152.9 44.4 all-gather.12
  203.2 41.6 all-reduce.6
  246.3 45.7 all-gather.14
where the time goes:
time: 313 us
  waiting for transfers between devices  227 us (73%)
  matrix products  24.5 us (8%)
  other arithmetic  20.6 us (7%)
  between operations  13.7 us (4%)
  blocking collectives  13 us (4%)
  starting transfers between devices  7.2 us (2%)
  local copies, waits for them, and re-layouts  6.35 us (2%)
    all_gather x2, waiting for transfers between devices, per_device(): whole_in = lax.all_gather(in_weight[layer_index], 'sp', axis=0, tiled=True)  82.1 us
    psum x2, waiting for transfers between devices, per_device(): hidden = lax.psum(partial_value.astype(jnp.bfloat16), 'tp')  81.1 us
    all_gather x2, waiting for transfers between devices, per_device(): lax.all_gather(out_weight[layer_index], 'sp', axis=0, tiled=True)  52.2 us
    psum x2, blocking collectives, per_device(): lax.psum((jnp.sum(summed, axis=1), jnp.sum(summed * summed, axis=1)), 'tp')  13 us
    dot_general x2, matrix products, per_device(): lax.dot_general(scaled, lax.all_gather(out_weight[layer_index], 'sp', axi...  11.4 us
    ppermute x2, waiting for transfers between devices, passed_along(): return lax.ppermute(block, axis, route)  10.9 us
    dot_general x2, matrix products, per_device(): lax.dot_general(whole_in, current, contract_cols, preferred_element_type=...  10.6 us
    convert_element_type x2, other arithmetic, pooled_windows(): (window_sums / counts - hidden.astype(jnp.float32)).astype(jnp.bfloat16)  8.26 us
  transfers between devices with their start and end apart: 8, of which 8 were waited for; matrix products, arithmetic and copies ran while one was open for 10% of the time, Pallas kernels for 0%

commit v1 on v0

v1 whole, which is shorter than its diff:
```python
import functools

import jax
import jax.numpy as jnp
from jax import lax
from jax.experimental import pallas as pl
from jax.experimental.pallas import tpu as pltpu
from jax.sharding import PartitionSpec as P

MESH = pl.DeviceIdType.MESH
EPSILON = 1e-05
F32 = jnp.float32
BF16 = jnp.bfloat16
REACH = 16
NT = (((1,), (1,)), ((), ()))


def arrival_orders(n):
    orders = []
    for z in range(n):
        first = 1 if z < n / 2 else -1
        order = [z]
        for d in range(1, n):
            order += [b for b in (z + first * d, z - first * d) if 0 <= b < n]
        orders.append(order)
    return orders


def kernel(cfg, *refs):
    n, tp_n, layers, groups, width, streamed = cfg
    (stream, w_in, w_out, mix, gain, norm_gain, norm_shift, out,
     wg, cur, acc, psend, precv, pown, xsend, xrecv, hbuf, hsend, hrecv, sc, tsend, trecv,
     loc_sem, own_send, f_send, z_recv, y_send, y_recv,
     p_send_s, p_recv_s, x_send_s, x_recv_s, h_send_s, h_recv_s,
     c_send_s, c_recv_s, t_send_s, t_recv_s, out_sem) = refs
    tokens, chans = cur.shape
    half = tokens // 2
    block = 256
    chunks = tokens // block
    d_model = chans * tp_n
    alpha = (2.0 * layers) ** 0.25
    nx = tp_n // 2
    y, z, t = lax.axis_index("grp"), lax.axis_index("sp"), lax.axis_index("tp")
    core, x = lax.rem(t, 2), t // 2
    sib = t + 1 - 2 * core
    orders = arrival_orders(n)
    mine, other = core * half, (1 - core) * half
    mine = pl.multiple_of(mine, half)
    other = pl.multiple_of(other, half)

    def order(s):
        if not streamed:
            return jnp.int32(s)
        b = jnp.int32(0)
        for k in range(n):
            b = jnp.where(z == k, orders[k][s], b)
        return b

    def remote(src, dst, ssem, rsem, device):
        return pltpu.make_async_remote_copy(
            src_ref=src, dst_ref=dst, send_sem=ssem, recv_sem=rsem,
            device_id=device, device_id_type=MESH)

    rows = w_in.shape[1]
    copies = [pltpu.make_async_copy(stream, cur, loc_sem.at[0])]
    for m in range(2 * layers):
        src = (w_in, w_out)[m % 2].at[m // 2]
        if streamed:
            dst = wg.at[m, pl.ds(pl.multiple_of(z * rows, rows), rows)]
        else:
            dst = wg.at[m]
        copies.append(pltpu.make_async_copy(src, dst, loc_sem.at[1 + m]))
    for copy in copies:
        copy.start()

    barrier = pltpu.get_barrier_semaphore()

    def greet(device):
        pl.semaphore_signal(barrier, inc=1, device_id=device, device_id_type=MESH)

    for k in range(1, tp_n):
        greet((y, z, lax.rem(t + k, tp_n)))
    count = jnp.int32(tp_n - 1)
    if streamed:
        greet((1 - y, z, t))
        count = count + 1

        @pl.when(z > 0)
        def _():
            greet((y, z - 1, t))

        @pl.when(z < n - 1)
        def _():
            greet((y, z + 1, t))

        count = count + jnp.where(z > 0, 1, 0) + jnp.where(z < n - 1, 1, 0)
    down = (core == 1) & (z < n - 1)
    up = (core == 0) & (z > 0)

    @pl.when(down)
    def _():
        greet((y, z + 1, sib))

    @pl.when(up)
    def _():
        greet((y, z - 1, sib))

    count = count + jnp.where(down, 1, 0) + jnp.where(up, 1, 0)
    pl.semaphore_wait(barrier, count)

    part = rows // 2

    def own_copy(m, side):
        src = (w_in, w_out)[m % 2].at[m // 2, pl.ds(pl.multiple_of(y * part, part), part)]
        dst = wg.at[m, pl.ds(pl.multiple_of(z * rows + y * part, part), part)]
        return remote(src, dst, own_send.at[m, side], z_recv.at[m, z], (y, z + 2 * side - 1, t))

    def own_each(m, what):
        for side in (1, 0):
            @pl.when(z < n - 1 if side else z > 0)
            def _(side=side):
                what(own_copy(m, side))

    def piece(m, b, from_y):
        return wg.at[m, pl.ds(pl.multiple_of(b * rows + from_y * part, part), part)]

    def onward(m, b):
        zt = jnp.where(b < z, z + 1, z - 1)
        ref = piece(m, b, y)
        return (zt >= 0) & (zt < n), remote(ref, ref, f_send.at[m, b], z_recv.at[m, b], (y, zt, t))

    def across(m, b, from_y):
        ref = piece(m, b, from_y)
        return remote(ref, ref, y_send.at[m, b], y_recv.at[m, b], (1 - y, z, t))

    events = [(m, s) for m in range(2 * layers) for s in range(1, n)]
    state = [0]

    def advance(m, s, ahead=0):
        if not streamed:
            return
        goal = min(m * (n - 1) + s + ahead, len(events))
        while state[0] < goal:
            em, es = events[state[0]]
            state[0] += 1
            b = order(es)
            there, copy = onward(em, b)
            copy.wait_recv()
            pl.when(there)(copy.start)
            across(em, b, y).start()
            if es == 2 and em + 2 < 2 * layers:
                own_each(em + 2, lambda c: c.start())

    def ready(m, s):
        if s == 0 or not streamed:
            if s == 0:
                copies[1 + m].wait()
        else:
            across(m, order(s), 1 - y).wait_recv()

    def weight(m, s):
        return wg[m, pl.ds(pl.multiple_of(order(s) * block, block), block), :]

    def p_copy(l, s):
        return remote(psend.at[l, s], precv.at[l, s], p_send_s.at[l, s], p_recv_s.at[l, s], (y, z, sib))

    def x_copies(l, s):
        return [remote(xsend.at[l, s], xrecv.at[k - 1, l, s], x_send_s.at[k - 1, l, s],
                       x_recv_s.at[k - 1, l, s], (y, z, lax.rem(x + k, nx) * 2 + core))
                for k in range(1, nx)]

    def h_copy(l, s):
        b = order(s)
        return remote(hsend.at[l, b], hrecv.at[l, b], h_send_s.at[l, b], h_recv_s.at[l, b],
                      (y, z + core, sib))

    def c_copy(l, s, at):
        ref = sc.at[l, s, pl.ds(at, half)]
        return remote(ref, ref, c_send_s.at[l, s], c_recv_s.at[l, s], (y, z, sib))

    def t_copies(l, i):
        return [remote(tsend.at[l, i], trecv.at[k - 1, l, i], t_send_s.at[k - 1, l, i],
                       t_recv_s.at[k - 1, l, i], (y, z, lax.rem(t + k, tp_n)))
                for k in range(1, tp_n)]

    h_out = (core == 0) | (z < n - 1)
    h_in = (core == 1) | (z > 0)

    def project(l, s):
        w = weight(2 * l, s)
        psend[l, s] = lax.dot_general(
            cur[pl.ds(other, half), :], w, NT, preferred_element_type=F32).astype(BF16)
        p_copy(l, s).start()
        pown[s] = lax.dot_general(cur[pl.ds(mine, half), :], w, NT, preferred_element_type=F32)

    def chip_sum(l, s):
        p_copy(l, s).wait_recv()
        total = pown[s] + precv[l, s].astype(F32)
        pown[s] = total
        xsend[l, s] = total.astype(BF16)
        for copy in x_copies(l, s):
            copy.start()

    def finish_hidden(l, s):
        total = pown[s]
        for k, copy in enumerate(x_copies(l, s)):
            copy.wait_recv()
            total = total + xrecv[k, l, s].astype(F32)
        hidden = total.astype(BF16)
        hbuf[s, REACH:, :] = hidden.astype(F32)
        hsend[l, order(s)] = hidden[half - REACH:, :]
        pl.when(h_out)(h_copy(l, s).start)

    def pool(l, s):
        b = order(s)

        @pl.when(h_in)
        def _():
            h_copy(l, s).wait_recv()
            hbuf[s, :REACH, :] = hrecv[l, b].astype(F32)

        @pl.when(jnp.logical_not(h_in))
        def _():
            hbuf[s, :REACH, :] = jnp.zeros((REACH, width), F32)

        ext = hbuf[s]
        run = ext + pltpu.roll(ext, 1, 0)
        for octave in range(1, groups):
            take = jnp.where(b >= octave, 1.0, 0.0).astype(F32)
            run = run + take * pltpu.roll(run, 2**octave, 0)
        reach = jnp.int32(2)
        for octave in range(1, groups):
            reach = jnp.where(b >= octave, 2 ** (octave + 1), reach)
        at = z * tokens + core * half + 1 + lax.broadcasted_iota(jnp.int32, (half, width), 0)
        counts = jnp.minimum(at, reach).astype(F32)
        pooled = (run[REACH:, :] / counts - ext[REACH:, :]).astype(BF16)
        mixed = jnp.dot(pooled, mix[l, b], preferred_element_type=F32)
        sc[l, s, pl.ds(mine, half), :] = (mixed * gain[l, b]).astype(BF16)
        c_copy(l, s, mine).start()

    def expand(l, s):
        c_copy(l, s, other).wait_recv()
        at_m = 2 * l + 1

        def body(i, carry):
            r = pl.ds(pl.multiple_of(i * block, block), block)
            add = jnp.dot(sc[l, s, r, :], weight(at_m, s), preferred_element_type=F32)
            if s == 0:
                acc[r, :] = alpha * cur[r, :].astype(F32) + add
            else:
                acc[r, :] = acc[r, :] + add
            return carry

        if s < groups - 1:
            lax.fori_loop(0, chunks, body, 0)
            return
        for i in range(chunks):
            body(i, 0)
            v = acc[i * block:(i + 1) * block, :]
            lane = lax.broadcasted_iota(jnp.int32, (block, 128), 1)
            row_sum = jnp.sum(v, axis=1, keepdims=True)
            row_squares = jnp.sum(v * v, axis=1, keepdims=True)
            both = jnp.where(lane == 0, row_sum, jnp.where(lane == 1, row_squares, 0.0))
            tsend[l, i] = both.T[:8, :]
            for copy in t_copies(l, i):
                copy.start()

    def norm(l):
        dst = out if l == layers - 1 else cur
        for i in range(chunks):
            stats = tsend[l, i]
            for k, copy in enumerate(t_copies(l, i)):
                copy.wait_recv()
                stats = stats + trecv[k, l, i]
            stats = stats / d_model
            mean = stats[0:1, :]
            var = stats[1:2, :] - mean * mean
            inv = lax.rsqrt(var + EPSILON)
            row = lax.broadcasted_iota(jnp.int32, (128, block), 0)
            cols = jnp.where(row == 0, mean, jnp.where(row == 1, inv, 0.0)).T
            r = slice(i * block, (i + 1) * block)
            v = (acc[r, :] - cols[:, 0:1]) * cols[:, 1:2]
            dst[r, :] = (v * norm_gain[l:l + 1, :] + norm_shift[l:l + 1, :]).astype(BF16)

    if streamed:
        own_each(0, lambda c: c.start())
        own_each(1, lambda c: c.start())
    copies[0].wait()
    last = groups - 1
    for l in range(layers):
        mi, mo = 2 * l, 2 * l + 1
        ready(mi, 0)
        project(l, 0)
        for s in range(1, groups):
            advance(mi, s, 1)
            chip_sum(l, s - 1)
            ready(mi, s)
            project(l, s)
        chip_sum(l, last)
        for s in range(groups):
            finish_hidden(l, s)
        advance(mo, 2)
        for s in range(groups):
            pool(l, s)
        ready(mo, 0)
        expand(l, 0)
        for s in range(1, groups):
            advance(mo, s, 1)
            ready(mo, s)
            expand(l, s)
        norm(l)

    if streamed:
        for m in range(2 * layers):
            own_each(m, lambda c: c.wait_send())
            for s in range(1, n):
                b = order(s)
                there, copy = onward(m, b)
                pl.when(there)(copy.wait_send)
                across(m, b, y).wait_send()
    for l in range(layers):
        for s in range(groups):
            p_copy(l, s).wait_send()
            for copy in x_copies(l, s):
                copy.wait_send()
            pl.when(h_out)(h_copy(l, s).wait_send)
            c_copy(l, s, mine).wait_send()
        for i in range(chunks):
            for copy in t_copies(l, i):
                copy.wait_send()


def per_device(n, grp_n, tp_n, stream, in_weight, out_weight, group_mix, pool_gain, norm_gain, norm_shift):
    layers, groups, width = group_mix.shape[:3]
    tokens, chans = stream.shape
    pool = groups * width
    streamed = n == groups and grp_n == 2
    if not streamed:
        in_weight = lax.all_gather(in_weight, "sp", axis=1, tiled=True)
        out_weight = lax.all_gather(out_weight, "sp", axis=1, tiled=True)
    nx = tp_n // 2
    half = tokens // 2
    chunks = tokens // 256
    ms = 2 * layers
    dma = pltpu.SemaphoreType.DMA
    any_spec = pl.BlockSpec(memory_space=pl.ANY)
    vmem = pl.BlockSpec(memory_space=pltpu.VMEM)
    xs = max(nx - 1, 1)
    return pl.pallas_call(
        functools.partial(kernel, (n, tp_n, layers, groups, width, streamed)),
        out_shape=jax.ShapeDtypeStruct((tokens, chans), BF16),
        in_specs=[any_spec] * 3 + [vmem] * 4,
        out_specs=vmem,
        scratch_shapes=[
            pltpu.VMEM((ms, pool, chans), BF16),
            pltpu.VMEM((tokens, chans), BF16),
            pltpu.VMEM((tokens, chans), F32),
            pltpu.VMEM((layers, groups, half, width), BF16),
            pltpu.VMEM((layers, groups, half, width), BF16),
            pltpu.VMEM((groups, half, width), F32),
            pltpu.VMEM((layers, groups, half, width), BF16),
            pltpu.VMEM((xs, layers, groups, half, width), BF16),
            pltpu.VMEM((groups, REACH + half, width), F32),
            pltpu.VMEM((layers, groups, REACH, width), BF16),
            pltpu.VMEM((layers, groups, REACH, width), BF16),
            pltpu.VMEM((layers, groups, tokens, width), BF16),
            pltpu.VMEM((layers, chunks, 8, 256), F32),
            pltpu.VMEM((tp_n - 1, layers, chunks, 8, 256), F32),
            dma((1 + ms,)),
            dma((ms, 2)), dma((ms, groups)), dma((ms, groups)), dma((ms, groups)), dma((ms, groups)),
            dma((layers, groups)), dma((layers, groups)),
            dma((xs, layers, groups)), dma((xs, layers, groups)),
            dma((layers, groups)), dma((layers, groups)),
            dma((layers, groups)), dma((layers, groups)),
            dma((tp_n - 1, layers, chunks)), dma((tp_n - 1, layers, chunks)),
            dma((1,)),
        ],
        compiler_params=pltpu.CompilerParams(
            collective_id=0, has_side_effects=True, vmem_limit_bytes=56 * 1024 * 1024),
    )(stream, in_weight, out_weight, group_mix,
      pool_gain.reshape(layers, groups, 1, width), norm_gain, norm_shift)


def solution(mesh):
    in_specs = (
        P(("grp", "sp"), "tp"),
        P(None, "sp", "tp"),
        P(None, "sp", "tp"),
        P(),
        P(),
        P(None, "tp"),
        P(None, "tp"),
    )
    out_specs = P(("grp", "sp"), "tp")
    sizes = mesh.shape
    body = functools.partial(per_device, sizes["sp"], sizes["grp"], sizes["tp"])
    return jax.shard_map(
        body, mesh=mesh, in_specs=in_specs, out_specs=out_specs, check_vma=False
    )
```

time: 313 us -> 124 us (0.40)
  waiting for transfers between devices: 227 us -> 0 us
  Pallas kernels: 0 us -> 120 us
  matrix products: 24.5 us -> 0 us
  other arithmetic: 20.6 us -> 0 us
  between operations: 13.7 us -> 0.01 us
  blocking collectives: 13 us -> 0 us
  starting transfers between devices: 7.2 us -> 0 us
    all_gather x4 -> x0, waiting for transfers between devices: 134 us -> none  [the longest x2 82.1 us: per_device(): whole_in = lax.all_gather(in_weight[layer_index], 'sp', axis=0, tiled=True)]
    pallas_call x0 -> x1, Pallas kernels: none -> 120 us  [per_device(): pl.pallas_call(functools.partial(kernel, (n, tp_n, layers, groups, width,...]
    psum x2 -> x0, waiting for transfers between devices: 81.1 us -> none  [per_device(): hidden = lax.psum(partial_value.astype(jnp.bfloat16), 'tp')]
    dot_general x6 -> x0, matrix products: 24.5 us -> none  [the longest x2 11.4 us: per_device(): lax.dot_general(scaled, lax.all_gather(out_weight[layer_index], 'sp', axi...]
    convert_element_type x6 -> x0, other arithmetic: 14.5 us -> none  [the longest x2 8.26 us: pooled_windows(): (window_sums / counts - hidden.astype(jnp.float32)).astype(jnp.bfloat16)]
    psum x2 -> x0, blocking collectives: 13 us -> none  [per_device(): lax.psum((jnp.sum(summed, axis=1), jnp.sum(summed * summed, axis=1)), 'tp')]
    ppermute x2 -> x0, waiting for transfers between devices: 10.9 us -> none  [passed_along(): return lax.ppermute(block, axis, route)]
    ppermute x2 -> x0, starting transfers between devices: 6.99 us -> none  [passed_along(): return lax.ppermute(block, axis, route)]
  transfers between devices with their start and end apart: 8 -> 0, of which waited for: 8 -> 0; matrix products, arithmetic and copies ran while one was open for 10% -> 0% of each run, Pallas kernels for 0% -> 0%
where the time goes in v1:
time: 124 us
  Pallas kernels  120 us (97%)
  local copies, waits for them, and re-layouts  3.98 us (3%)
    pallas_call x1, Pallas kernels, per_device(): pl.pallas_call(functools.partial(kernel, (n, tp_n, layers, groups, width,...  120 us
    unnamed x1, local copies, waits for them, and re-layouts  2.67 us

profile of v1, /device:TPU:0, one launch (start us, length us, event | category | flops | bytes accessed | tf_op | source)
XLA Modules:
  0.0 124.2 jit_solution(12671603821797298167)
XLA Ops:
  0.0 1.3 %reshape.3.refs_4_ = f32[2,4,1,256]{3,2,1,0:T(1,128)} reshape(f32[2,1024]{1,0:T(2,128)} %param.11) | data formatting | bytes 16384 | tf_op jit(solution)/shard_map/reshape | solution.py:381
  1.3 120.2 %shard_map.73 = bf16[768,1024]{1,0:T(8,128)(2,1)} custom-call(bf16[768,1024]{1,0:T(8,128)(2,1)} %refs_0_.1, bf16[2,256,1024]{2,1,0:T(8,128)(2,1)} %refs_1_.1, bf16[2,256,1024]{2,1,0:T(8,128)(2,1)} %refs_2_.1, bf16[2,4,256,256]{3,2,1,0:T(8,128)(2,1)} %refs_3_.1, f32[2,4,1,256]{3,2,1,0:T(1,128)} %reshape.3.refs_4_, f32[2,1024]{1,0:T(2,128)} %refs_5_.1, ...), custom_call_target="tpu_custom_call" | custom-call | tf_op jit(solution)/shard_map/pallas_call | solution.py:349
  121.5 2.7 %copy.9 = bf16[768,1024]{1,0:T(8,128)(2,1)} copy(bf16[768,1024]{1,0:T(8,128)(2,1)} %shard_map.73) | data formatting | bytes 3145728

commit v2 on v1

--- a/solution.py
+++ b/solution.py
@@ -12,6 +12,7 @@
 F32 = jnp.float32
 BF16 = jnp.bfloat16
 REACH = 16
+PIECES = 2
 NT = (((1,), (1,)), ((), ()))
 
 
@@ -109,54 +110,63 @@
     pl.semaphore_wait(barrier, count)
 
     part = rows // 2
-
-    def own_copy(m, side):
-        src = (w_in, w_out)[m % 2].at[m // 2, pl.ds(pl.multiple_of(y * part, part), part)]
-        dst = wg.at[m, pl.ds(pl.multiple_of(z * rows + y * part, part), part)]
-        return remote(src, dst, own_send.at[m, side], z_recv.at[m, z], (y, z + 2 * side - 1, t))
-
-    def own_each(m, what):
-        for side in (1, 0):
-            @pl.when(z < n - 1 if side else z > 0)
-            def _(side=side):
-                what(own_copy(m, side))
-
-    def piece(m, b, from_y):
-        return wg.at[m, pl.ds(pl.multiple_of(b * rows + from_y * part, part), part)]
-
-    def onward(m, b):
+    cut = part // PIECES
+
+    def span(base, q):
+        return pl.ds(pl.multiple_of(base + q * cut, cut), cut)
+
+    def own_copy(m, side, q):
+        src = (w_in, w_out)[m % 2].at[m // 2, span(y * part, q)]
+        dst = wg.at[m, span(z * rows + y * part, q)]
+        return remote(src, dst, own_send.at[m, side, q], z_recv.at[m, z, q], (y, z + 2 * side - 1, t))
+
+    def own_side(m, side, when, what):
+        @pl.when(when & (z < n - 1 if side else z > 0))
+        def _():
+            for q in range(PIECES):
+                what(own_copy(m, side, q))
+
+    def onward(m, b, q):
         zt = jnp.where(b < z, z + 1, z - 1)
-        ref = piece(m, b, y)
-        return (zt >= 0) & (zt < n), remote(ref, ref, f_send.at[m, b], z_recv.at[m, b], (y, zt, t))
-
-    def across(m, b, from_y):
-        ref = piece(m, b, from_y)
-        return remote(ref, ref, y_send.at[m, b], y_recv.at[m, b], (1 - y, z, t))
-
-    events = [(m, s) for m in range(2 * layers) for s in range(1, n)]
+        ref = wg.at[m, span(b * rows + y * part, q)]
+        return (zt >= 0) & (zt < n), remote(
+            ref, ref, f_send.at[m, b, q], z_recv.at[m, b, q], (y, zt, t))
+
+    def across(m, b, from_y, q):
+        ref = wg.at[m, span(b * rows + from_y * part, q)]
+        return remote(ref, ref, y_send.at[m, b, q], y_recv.at[m, b, q], (1 - y, z, t))
+
+    events = [(m, s, q) for m in range(2 * layers) for s in range(1, n) for q in range(PIECES)]
     state = [0]
+
+    def forwards_end(k, side):
+        steps = [s for s in range(1, n) if (orders[k][s] < k if side else orders[k][s] > k)]
+        return max(steps, default=0)
 
     def advance(m, s, ahead=0):
         if not streamed:
             return
-        goal = min(m * (n - 1) + s + ahead, len(events))
+        goal = min((m * (n - 1) + s) * PIECES + ahead, len(events))
         while state[0] < goal:
-            em, es = events[state[0]]
+            em, es, q = events[state[0]]
             state[0] += 1
             b = order(es)
-            there, copy = onward(em, b)
+            there, copy = onward(em, b, q)
             copy.wait_recv()
             pl.when(there)(copy.start)
-            across(em, b, y).start()
-            if es == 2 and em + 2 < 2 * layers:
-                own_each(em + 2, lambda c: c.start())
+            across(em, b, y, q).start()
+            if q == PIECES - 1 and em + 1 < 2 * layers:
+                for side in (1, 0):
+                    places = [k for k in range(n) if forwards_end(k, side) == es]
+                    for k in places:
+                        own_side(em + 1, side, z == k, lambda c: c.start())
 
     def ready(m, s):
-        if s == 0 or not streamed:
-            if s == 0:
-                copies[1 + m].wait()
-        else:
-            across(m, order(s), 1 - y).wait_recv()
+        if s == 0:
+            copies[1 + m].wait()
+        elif streamed:
+            for q in range(PIECES):
+                across(m, order(s), 1 - y, q).wait_recv()
 
     def weight(m, s):
         return wg[m, pl.ds(pl.multiple_of(order(s) * block, block), block), :]
@@ -235,7 +245,7 @@
         counts = jnp.minimum(at, reach).astype(F32)
         pooled = (run[REACH:, :] / counts - ext[REACH:, :]).astype(BF16)
         mixed = jnp.dot(pooled, mix[l, b], preferred_element_type=F32)
-        sc[l, s, pl.ds(mine, half), :] = (mixed * gain[l, b]).astype(BF16)
+        sc[l, s, pl.ds(mine, half), :] = (mixed * gain[l:l + 1, pl.ds(pl.multiple_of(b * width, width), width)]).astype(BF16)
         c_copy(l, s, mine).start()
 
     def expand(l, s):
@@ -283,8 +293,10 @@
             dst[r, :] = (v * norm_gain[l:l + 1, :] + norm_shift[l:l + 1, :]).astype(BF16)
 
     if streamed:
-        own_each(0, lambda c: c.start())
-        own_each(1, lambda c: c.start())
+        for m in range(2 * layers):
+            for side in (1, 0):
+                first = (z >= 0) if m == 0 else (z == 0 if side else z == n - 1)
+                own_side(m, side, first, lambda c: c.start())
     copies[0].wait()
     last = groups - 1
     for l in range(layers):
@@ -292,32 +304,36 @@
         ready(mi, 0)
         project(l, 0)
         for s in range(1, groups):
-            advance(mi, s, 1)
+            advance(mi, s, 2)
             chip_sum(l, s - 1)
             ready(mi, s)
             project(l, s)
         chip_sum(l, last)
         for s in range(groups):
             finish_hidden(l, s)
+        pool(l, 0)
+        pool(l, 1)
         advance(mo, 2)
-        for s in range(groups):
+        for s in range(2, groups):
             pool(l, s)
         ready(mo, 0)
         expand(l, 0)
         for s in range(1, groups):
-            advance(mo, s, 1)
+            advance(mo, s, 2)
             ready(mo, s)
             expand(l, s)
         norm(l)
 
     if streamed:
         for m in range(2 * layers):
-            own_each(m, lambda c: c.wait_send())
+            for side in (1, 0):
+                own_side(m, side, z >= 0, lambda c: c.wait_send())
             for s in range(1, n):
                 b = order(s)
-                there, copy = onward(m, b)
-                pl.when(there)(copy.wait_send)
-                across(m, b, y).wait_send()
+                for q in range(PIECES):
+                    there, copy = onward(m, b, q)
+                    pl.when(there)(copy.wait_send)
+                    across(m, b, y, q).wait_send()
     for l in range(layers):
         for s in range(groups):
             p_copy(l, s).wait_send()
@@ -367,7 +383,8 @@
             pltpu.VMEM((layers, chunks, 8, 256), F32),
             pltpu.VMEM((tp_n - 1, layers, chunks, 8, 256), F32),
             dma((1 + ms,)),
-            dma((ms, 2)), dma((ms, groups)), dma((ms, groups)), dma((ms, groups)), dma((ms, groups)),
+            dma((ms, 2, PIECES)), dma((ms, groups, PIECES)), dma((ms, groups, PIECES)),
+            dma((ms, groups, PIECES)), dma((ms, groups, PIECES)),
             dma((layers, groups)), dma((layers, groups)),
             dma((xs, layers, groups)), dma((xs, layers, groups)),
             dma((layers, groups)), dma((layers, groups)),
@@ -378,7 +395,7 @@
         compiler_params=pltpu.CompilerParams(
             collective_id=0, has_side_effects=True, vmem_limit_bytes=56 * 1024 * 1024),
     )(stream, in_weight, out_weight, group_mix,
-      pool_gain.reshape(layers, groups, 1, width), norm_gain, norm_shift)
+      pool_gain, norm_gain, norm_shift)
 
 
 def solution(mesh):

time: 124 us -> 112 us (0.903)
  Pallas kernels: 120 us -> 109 us
  local copies, waits for them, and re-layouts: 3.98 us -> 2.67 us
    pallas_call x1, Pallas kernels: 120 us -> 109 us  [per_device(): pl.pallas_call(functools.partial(kernel, (n, tp_n, layers, groups, width,...]
    reshape x1 -> x0, local copies, waits for them, and re-layouts: 1.31 us -> none  [per_device(): pool_gain.reshape(layers, groups, 1, width)]
where the time goes in v2:
time: 112 us
  Pallas kernels  109 us (97%)
  local copies, waits for them, and re-layouts  2.67 us (2%)
    pallas_call x1, Pallas kernels, per_device(): pl.pallas_call(functools.partial(kernel, (n, tp_n, layers, groups, width,...  109 us
    unnamed x1, local copies, waits for them, and re-layouts  2.67 us

profile of v2, /device:TPU:0, one launch (start us, length us, event | category | flops | bytes accessed | tf_op | source)
XLA Modules:
  0.0 111.6 jit_solution(12441114969377999901)
XLA Ops:
  0.0 108.9 %shard_map.73 = bf16[768,1024]{1,0:T(8,128)(2,1)} custom-call(bf16[768,1024]{1,0:T(8,128)(2,1)} %refs_0_.1, bf16[2,256,1024]{2,1,0:T(8,128)(2,1)} %refs_1_.1, bf16[2,256,1024]{2,1,0:T(8,128)(2,1)} %refs_2_.1, bf16[2,4,256,256]{3,2,1,0:T(8,128)(2,1)} %refs_3_.1, f32[2,1024]{1,0:T(2,128)} %refs_4_.1, f32[2,1024]{1,0:T(2,128)} %refs_5_.1, f32[2,1024]{1,0:T(2,128)} %refs_6_.1), custom_call_target="tpu_custom_call" | custom-call | tf_op jit(solution)/shard_map/pallas_call | solution.py:365
  108.9 2.7 %copy.9 = bf16[768,1024]{1,0:T(8,128)(2,1)} copy(bf16[768,1024]{1,0:T(8,128)(2,1)} %shard_map.73) | data formatting | bytes 3145728

commit v3 on v2

--- a/solution.py
+++ b/solution.py
@@ -304,7 +304,7 @@
         ready(mi, 0)
         project(l, 0)
         for s in range(1, groups):
-            advance(mi, s, 2)
+            advance(mi, s, 4)
             chip_sum(l, s - 1)
             ready(mi, s)
             project(l, s)
@@ -319,7 +319,7 @@
         ready(mo, 0)
         expand(l, 0)
         for s in range(1, groups):
-            advance(mo, s, 2)
+            advance(mo, s, 4)
             ready(mo, s)
             expand(l, s)
         norm(l)

time: 112 us -> 113 us (level)
  no operation moved by 1% of the time
where the time goes in v3:
time: 113 us; the launch traced here: 112 us
  Pallas kernels  110 us (97%)
  local copies, waits for them, and re-layouts  2.67 us (2%)
    pallas_call x1, Pallas kernels, per_device(): pl.pallas_call(functools.partial(kernel, (n, tp_n, layers, groups, width,...  110 us
    unnamed x1, local copies, waits for them, and re-layouts  2.67 us

profile of v3, /device:TPU:0, one launch (start us, length us, event | category | flops | bytes accessed | tf_op | source)
XLA Modules:
  0.0 112.5 jit_solution(11856914528940697090)
XLA Ops:
  0.0 109.8 %shard_map.73 = bf16[768,1024]{1,0:T(8,128)(2,1)} custom-call(bf16[768,1024]{1,0:T(8,128)(2,1)} %refs_0_.1, bf16[2,256,1024]{2,1,0:T(8,128)(2,1)} %refs_1_.1, bf16[2,256,1024]{2,1,0:T(8,128)(2,1)} %refs_2_.1, bf16[2,4,256,256]{3,2,1,0:T(8,128)(2,1)} %refs_3_.1, f32[2,1024]{1,0:T(2,128)} %refs_4_.1, f32[2,1024]{1,0:T(2,128)} %refs_5_.1, f32[2,1024]{1,0:T(2,128)} %refs_6_.1), custom_call_target="tpu_custom_call" | custom-call | tf_op jit(solution)/shard_map/pallas_call | solution.py:365
  109.8 2.7 %copy.9 = bf16[768,1024]{1,0:T(8,128)(2,1)} copy(bf16[768,1024]{1,0:T(8,128)(2,1)} %shard_map.73) | data formatting | bytes 3145728
